TPU v7x, 32 devices: a whole 2x2x4 slice. The times are simulated.
32 devices in a mesh: st: 4 (over y, x), tp: 8 (over z, core).
Axes of the slice: x: 2, y: 2, z: 4, core: 2. Of those that a mesh axis runs over, the one named last changes fastest.
Arguments:
- normed: bfloat16 [2048, 2048], P('st'), may hold values from -128 to 128
- store: bfloat16 [8192, 2048], P('st'), may hold values from -5 to 5
- passage_ids: int32 [16, 2], P('st'), may hold values from 0 to 127, as said below
- w_query: bfloat16 [2048, 2048], P(None, 'tp'), as said below
- w_gate: bfloat16 [2048, 2048], P(None, 'tp'), may hold values from -0.125 to 0.125
- w_key: bfloat16 [2048, 2048], P(None, 'tp'), as said below
- w_value: bfloat16 [2048, 2048], P(None, 'tp'), may hold values from -0.125 to 0.125
- cotangent: bfloat16 [2048, 2048], P('st', 'tp'), may hold values from -6 to 6
Outputs:
- grad_rows: float32 [2048, 2048], P('st', 'tp')
- grad_store: float32 [8192, 2048], P('st', 'tp')
- grad_query_weight: float32 [2048, 2048], P('st', 'tp')
Inputs may be any that keep to these rules, and one draw needn't show every extreme that they name: `passage_ids`: each row names 2 passages. The passages read by the blocks of one index of st are all different, and at most 4 of them belong to any one owner (the owner of passage p is the index p // 32 of st). In every draw some owner has one of its passages read by every index of st. `w_query`: entries lie within 6 * 2048 ** -0.5 in magnitude. `w_key`: entries lie within 8 * 2048 ** -0.5 in magnitude.
All inputs are finite; a program needn't handle non-finite values.
Results may differ from a plain program's by a relative error of at most 0.019.
Values may be sent and summed in bfloat16 or wider, within the bound.
A program may use at most 128 MiB of HBM per device.

v0:
```python
import jax
import jax.numpy as jnp
from jax import lax
from jax.sharding import PartitionSpec as P

DH = 128
BLK = 128
PLEN = 64


def shards(normed, store, passage_ids, w_query, w_gate, w_key, w_value, cotangent):
    peer_count = lax.axis_size("st")
    blocks = passage_ids.shape[0]
    read_count = passage_ids.shape[1]
    requests = blocks * read_count
    slot_most = max(1, 2 * requests // peer_count)
    slot_count = peer_count * slot_most
    tok_rows = normed.shape[0]
    head_width = w_query.shape[1]
    heads_dev = head_width // DH
    pass_dev = store.shape[0] // PLEN
    key_span = read_count * PLEN
    score_scale = DH ** (-0.5)
    flat_ids = passage_ids.reshape(requests)
    owners = flat_ids // pass_dev
    local_ids = flat_ids % pass_dev
    positions = jnp.arange(requests, dtype=jnp.int32)
    before = (owners[:, None] == owners[None, :]) & (positions[None, :] < positions[:, None])
    rank_among = jnp.sum(before.astype(jnp.int32), axis=1)
    slot_of = owners * slot_most + rank_among
    slot_hit = slot_of[:, None] == jnp.arange(slot_count, dtype=jnp.int32)[None, :]
    slot_table = jnp.max(jnp.where(slot_hit, local_ids[:, None], -1), axis=0)
    wanted = lax.all_to_all(
        slot_table.reshape(peer_count, slot_most), "st", split_axis=0, concat_axis=0, tiled=True
    )
    w_pair = jnp.concatenate([w_key, w_value], axis=1)
    projected = jnp.dot(store, w_pair, preferred_element_type=jnp.float32).astype(jnp.bfloat16)
    projected = projected.reshape(pass_dev, PLEN, 2 * head_width)
    served_ids = wanted.reshape(slot_count)
    served = jnp.take(projected, jnp.maximum(served_ids, 0), axis=0)
    served = jnp.where((served_ids >= 0)[:, None, None], served, jnp.zeros_like(served))
    arrived = lax.all_to_all(
        served.reshape(peer_count, slot_most, PLEN, 2 * head_width),
        "st",
        split_axis=0,
        concat_axis=0,
        tiled=True,
    )
    queries = jnp.dot(normed, w_query, preferred_element_type=jnp.float32).astype(jnp.bfloat16)
    gate_open = jax.nn.sigmoid(jnp.dot(normed, w_gate, preferred_element_type=jnp.float32))
    picked = jnp.take(arrived.reshape(slot_count, PLEN, 2 * head_width), slot_of, axis=0)
    picked = picked.reshape(blocks, key_span, 2, heads_dev, DH)
    key_rows = picked[:, :, 0]
    value_rows = picked[:, :, 1]
    q_blocks = queries.reshape(blocks, BLK, heads_dev, DH)
    scores = (
        jnp.einsum("bthd,bshd->bhts", q_blocks, key_rows, preferred_element_type=jnp.float32)
        * score_scale
    )
    attn_probs = jax.nn.softmax(scores, axis=-1)
    probs_low = attn_probs.astype(jnp.bfloat16)
    attended = jnp.einsum(
        "bhts,bshd->bthd", probs_low, value_rows, preferred_element_type=jnp.float32
    )
    gate_blocks = gate_open.reshape(blocks, BLK, heads_dev, DH)
    upstream = cotangent.astype(jnp.float32).reshape(blocks, BLK, heads_dev, DH)
    d_attended = (upstream * gate_blocks).astype(jnp.bfloat16)
    d_gate = (upstream * attended * gate_blocks * (1.0 - gate_blocks)).astype(jnp.bfloat16)
    d_gate = d_gate.reshape(tok_rows, head_width)
    d_values = jnp.einsum(
        "bhts,bthd->bshd", probs_low, d_attended, preferred_element_type=jnp.float32
    ).astype(jnp.bfloat16)
    d_probs = jnp.einsum(
        "bthd,bshd->bhts", d_attended, value_rows, preferred_element_type=jnp.float32
    )
    row_delta = jnp.sum(d_probs * attn_probs, axis=-1, keepdims=True)
    d_scores = (attn_probs * (d_probs - row_delta) * score_scale).astype(jnp.bfloat16)
    d_query = (
        jnp.einsum("bhts,bshd->bthd", d_scores, key_rows, preferred_element_type=jnp.float32)
        .astype(jnp.bfloat16)
        .reshape(tok_rows, head_width)
    )
    d_keys = jnp.einsum(
        "bhts,bthd->bshd", d_scores, q_blocks, preferred_element_type=jnp.float32
    ).astype(jnp.bfloat16)
    d_pair = jnp.stack([d_keys, d_values], axis=2).reshape(requests, PLEN, 2 * head_width)
    row_part = jnp.dot(d_query, w_query.T, preferred_element_type=jnp.float32)
    row_part = row_part + jnp.dot(d_gate, w_gate.T, preferred_element_type=jnp.float32)
    grad_query_weight = lax.psum_scatter(
        lax.dot_general(
            normed, d_query, (((0,), (0,)), ((), ())), preferred_element_type=jnp.float32
        ).astype(jnp.bfloat16),
        "st",
        scatter_dimension=0,
        tiled=True,
    ).astype(jnp.float32)
    owned = (jnp.arange(pass_dev, dtype=jnp.int32)[:, None] == served_ids[None, :]).astype(
        jnp.float32
    )
    per_request = jnp.dot(
        d_pair.reshape(requests * PLEN, 2 * head_width),
        w_pair.T,
        preferred_element_type=jnp.float32,
    )
    grad_rows, slice_part = (
        lax.psum_scatter(
            row_part.astype(jnp.bfloat16), "tp", scatter_dimension=1, tiled=True
        ).astype(jnp.float32),
        lax.psum_scatter(
            per_request.astype(jnp.bfloat16), "tp", scatter_dimension=1, tiled=True
        ).astype(jnp.float32),
    )
    slice_cols = slice_part.shape[1]
    outgoing = lax.dot_general(
        slot_hit.astype(jnp.float32),
        slice_part.reshape(requests, PLEN * slice_cols),
        (((0,), (0,)), ((), ())),
        precision=lax.Precision.HIGHEST,
    )
    returned = lax.all_to_all(
        outgoing.reshape(peer_count, slot_most, PLEN, slice_cols).astype(jnp.bfloat16),
        "st",
        split_axis=0,
        concat_axis=0,
        tiled=True,
    ).astype(jnp.float32)
    grad_store = jnp.dot(
        owned, returned.reshape(slot_count, PLEN * slice_cols), precision=lax.Precision.HIGHEST
    ).reshape(pass_dev * PLEN, slice_cols)
    return (grad_rows, grad_store, grad_query_weight)


def solution(mesh):
    placed = (
        P("st", None),
        P("st", None),
        P("st", None),
        P(None, "tp"),
        P(None, "tp"),
        P(None, "tp"),
        P(None, "tp"),
        P("st", "tp"),
    )
    return jax.shard_map(
        shards,
        mesh=mesh,
        in_specs=placed,
        out_specs=(P("st", "tp"), P("st", "tp"), P("st", "tp")),
        check_vma=False,
    )
```

profile of v0, /device:TPU:0, one launch (start us, length us, event | category | flops | bytes accessed | tf_op | source)
XLA Modules:
  0.0 202.9 jit_solution(8173390940594196393)
XLA Ops:
  9.2 5.2 %all-to-all-start = ((s32[4,1,4]{2,1,0:T(1,128)}), s32[4,1,4]{2,1,0:T(1,128)S(1)}, u32[]{:S(2)}, u32[]{:S(2)}) async-start(s32[4,1,4]{2,1,0:T(1,128)} %bitcast), calls=%async_computation | async-start | bytes 4096 | tf_op jit(solution)/shard_map/all_to_all | solution.py:33
  15.9 1.3 copy-done.8
  17.3 9.3 %fusion.2 = bf16[2048,512]{0,1:T(8,128)(2,1)} fusion(bf16[2048,512]{1,0:T(8,128)(2,1)S(1)} %constant_dynamic-update-slice_fusion, bf16[2048,2048]{1,0:T(8,128)(2,1)} %param.9), kind=kOutput, calls=%fused_computation.7 | convolution fusion | flops 4296015872 | bytes 12582912 | tf_op jit(solution)/shard_map/dot_general | solution.py:37
  26.6 4.0 %copy.116 = bf16[2048,512]{1,0:T(8,128)(2,1)} copy(bf16[2048,512]{0,1:T(8,128)(2,1)} %fusion.2) | data formatting | bytes 4194304 | tf_op jit(solution)/shard_map/convert_element_type | solution.py:37
  30.8 1.5 fusion.8
  35.2 3.2 %gather_fusion = bf16[16,64,512]{2,1,0:T(8,128)(2,1)} fusion(bf16[32,64,512]{2,1,0:T(8,128)(2,1)} %bitcast.104, s32[1024]{0:T(1024)S(1)} %pad_clamp_fusion.1), kind=kCustom, calls=%fused_computation | custom fusion | bytes 2097216 | tf_op jit(solution)/shard_map/jit(_take)/gather | solution.py:40
  38.4 2.4 %select_select_fusion = bf16[4,4,64,512]{3,2,1,0:T(8,128)(2,1)} fusion(bf16[4,4,64,512]{3,2,1,0:T(8,128)(2,1)} %bitcast.105, pred[4,4]{1,0:T(4,128)(4,1)S(1)} %get-tuple-element.26, pred[4,4]{1,0:T(4,128)(4,1)S(1)} %get-tuple-element.27), kind=kLoop, calls=%fused_computation.34 | loop fusion | flops 1048576 | bytes 2097184 | tf_op jit(solution)/shard_map/jit(_where)/select_n | solution.py:41
  40.8 4.3 %all-to-all-start.1 = ((bf16[4,4,64,512]{3,2,1,0:T(8,128)(2,1)}), bf16[4,4,64,512]{3,2,1,0:T(8,128)(2,1)}, u32[]{:S(2)}, u32[]{:S(2)}) async-start(bf16[4,4,64,512]{3,2,1,0:T(8,128)(2,1)} %select_select_fusion), calls=%async_computation.1 | async-start | bytes 2097152 | tf_op jit(solution)/shard_map/all_to_all | solution.py:42
  46.2 2.6 %convolution_convert_fusion.7 = bf16[512,256]{1,0:T(8,128)(2,1)} fusion(bf16[512,2048]{1,0:T(8,128)(2,1)S(1)} %copy-done, bf16[2048,256]{1,0:T(8,128)(2,1)} %param.11), kind=kOutput, calls=%fused_computation.30 | convolution fusion | flops 537001984 | bytes 3407872 | tf_op jit(solution)/shard_map/dot_general | solution.py:49
  50.8 8.0 %all-to-all-done.1 = bf16[4,4,64,512]{3,2,1,0:T(8,128)(2,1)} async-done(((bf16[4,4,64,512]{3,2,1,0:T(8,128)(2,1)}), bf16[4,4,64,512]{3,2,1,0:T(8,128)(2,1)}, u32[]{:S(2)}, u32[]{:S(2)}) %all-to-all-start.1) | async-done | bytes 1048608 | tf_op jit(solution)/shard_map/all_to_all | solution.py:42
  58.7 2.6 %gather_fusion.1 = bf16[8,64,512]{2,1,0:T(8,128)(2,1)} fusion(bf16[16,64,512]{2,1,0:T(8,128)(2,1)} %bitcast.4, s32[1024]{0:T(1024)S(1)} %pad_clamp_fusion), kind=kCustom, calls=%fused_computation.1 | custom fusion | bytes 1048608 | tf_op jit(solution)/shard_map/jit(_take)/gather | solution.py:51
  61.3 2.0 gather.15
  66.3 2.1 %fusion.55 = (f32[4,2,128]{2,1,0:T(2,128)S(1)}, f32[4,2,128,128]{2,3,1,0:T(8,128)}) fusion(bf16[4,128,2,128]{1,3,2,0:T(8,128)(2,1)} %copy.130, bf16[4,128,2,2,128]{4,1,3,0,2:T(8,128)(2,1)} %copy-done.1), kind=kOutput, calls=%fused_computation.109 | convolution fusion | flops 33947776 | bytes 1052672 | tf_op jit(solution)/shard_map/sub | solution.py:60
  68.4 2.3 %fusion.19 = bf16[4,128,1,2,128]{1,4,3,0,2:T(8,128)(2,1)} fusion(bf16[4,128,2,128]{1,3,2,0:T(8,128)(2,1)S(1)} %copy-done.3, f32[4,2,128]{2,1,0:T(2,128)S(1)} %get-tuple-element.24, bf16[4,128,2,128]{1,3,2,0:T(8,128)(2,1)} %copy.130, bf16[4,128,2,2,128]{4,1,3,0,2:T(8,128)(2,1)} %copy-done.1), kind=kOutput, calls=%fused_computation.33 | convolution fusion | flops 67765376 | bytes 1052672 | tf_op jit(solution)/shard_map/bhts,bthd->bshd/dot_general | solution.py:70
  70.7 2.7 %fusion.18 = bf16[4,128,1,2,128]{1,4,3,0,2:T(8,128)(2,1)} fusion(bf16[4,128,2,128]{1,3,2,0:T(8,128)(2,1)} %copy.130, f32[4,2,128,128]{2,3,1,0:T(8,128)} %fusion.31, f32[4,2,128,128]{2,3,1,0:T(8,128)} %get-tuple-element.25, f32[4,2,128]{2,1,0:T(2,128)S(1)} %get-tuple-element.24), kind=kOutput, calls=%fused_computation.32 | convolution fusion | flops 34604160 | bytes 1576960 | tf_op jit(solution)/shard_map/bhts,bthd->bshd/dot_general | solution.py:83
  73.3 1.8 pad_maximum_fusion
  75.1 2.0 copy.134
  77.2 2.0 %reshape_reshape.3 = bf16[512,512]{1,0:T(8,128)(2,1)} reshape(bf16[4,128,2,2,128]{4,3,2,1,0:T(2,128)(2,1)} %copy.134) | data formatting | bytes 1048576 | tf_op jit(solution)/shard_map/reshape;reshape | solution.py:101
  79.2 4.3 %convolution_convert_fusion = bf16[512,2048]{1,0:T(8,128)(2,1)} fusion(bf16[512,512]{1,0:T(8,128)(2,1)} %reshape_reshape.3, bf16[2048,512]{1,0:T(8,128)(2,1)} %copy-done.8), kind=kOutput, calls=%fused_computation.5 | convolution fusion | flops 1074790400 | bytes 4718592 | tf_op jit(solution)/shard_map/dot_general | solution.py:100
  83.6 2.7 %fusion.17 = bf16[4,128,2,128]{1,3,2,0:T(8,128)(2,1)} fusion(f32[4,2,128,128]{2,3,1,0:T(8,128)} %fusion.31, bf16[4,128,2,2,128]{4,1,3,0,2:T(8,128)(2,1)} %copy-done.1, f32[4,2,128,128]{2,3,1,0:T(8,128)} %get-tuple-element.25, f32[4,2,128]{2,1,0:T(2,128)S(1)} %get-tuple-element.24), kind=kOutput, calls=%fused_computation.31 | convolution fusion | flops 34604160 | bytes 2629632 | tf_op jit(solution)/shard_map/bhts,bshd->bthd/dot_general | solution.py:79
  87.4 1.7 fusion.3
  91.4 2.7 %fusion.16 = bf16[4,128,2,128]{1,3,2,0:T(8,128)(2,1)} fusion(f32[4,128,2,128]{1,3,2,0:T(8,128)} %copy.127, f32[4,128,2,128]{1,3,2,0:T(8,128)} %copy.126, bf16[4,128,2,2,128]{4,1,3,0,2:T(8,128)(2,1)} %copy-done.1, f32[4,2,128]{2,1,0:T(2,128)S(1)} %get-tuple-element.24, bf16[4,128,2,128]{1,3,2,0:T(8,128)(2,1)} %copy.130), kind=kOutput, calls=%fused_computation.26 | convolution fusion | flops 68289664 | bytes 2101248 | tf_op jit(solution)/shard_map/bhts,bshd->bthd/dot_general | solution.py:62
  94.1 1.8 copy.129
  97.2 2.1 %add_convert_fusion = bf16[512,2048]{1,0:T(8,128)(2,1)} fusion(f32[512,2048]{1,0:T(8,128)S(1)} %fusion.27, bf16[2048,256]{1,0:T(8,128)(2,1)S(1)} %copy-done.6, bf16[64,8,2,128]{3,2,1,0:T(2,128)(2,1)S(1)} %bitcast.111), kind=kOutput, calls=%fused_computation.4 | convolution fusion | flops 538968064 | bytes 7602176 | tf_op jit(solution)/shard_map/dot_general | solution.py:88
  99.3 20.8 %reduce-scatter.6.cloned.1.call-done = bf16[512,256]{1,0:T(8,128)(2,1)} async-done(((bf16[512,2048]{1,0:T(8,128)(2,1)}), bf16[512,256]{1,0:T(8,128)(2,1)}) %reduce-scatter.6.cloned.1.call-update) | async-done | bytes 262160 | tf_op jit(solution)/shard_map/reduce_scatter | solution.py:109
  122.3 3.6 %all-to-all-start.2 = ((bf16[4,4,64,256]{3,1,2,0:T(4,128)(2,1)}), bf16[4,4,64,256]{3,1,2,0:T(4,128)(2,1)S(1)}, u32[]{:S(2)}, u32[]{:S(2)}) async-start(bf16[4,4,64,256]{3,1,2,0:T(4,128)(2,1)} %convolution_convert_fusion.3), calls=%async_computation.4 | async-start | bytes 1048576 | tf_op jit(solution)/shard_map/all_to_all | solution.py:120
  126.0 24.7 %reduce-scatter.8.cloned.1.call-done = bf16[512,256]{0,1:T(8,128)(2,1)} async-done(((bf16[2048,256]{0,1:T(8,128)(2,1)}), bf16[512,256]{0,1:T(8,128)(2,1)}) %reduce-scatter.8.cloned.1.call-update) | async-done | bytes 262160 | tf_op jit(solution)/shard_map/reduce_scatter | solution.py:89
  150.7 1.9 copy.136
  152.6 37.1 %reduce-scatter.4.cloned.1.call-done = bf16[512,256]{1,0:T(8,128)(2,1)} async-done(((bf16[512,2048]{1,0:T(8,128)(2,1)}), bf16[512,256]{1,0:T(8,128)(2,1)}) %reduce-scatter.4.cloned.1.call-update) | async-done | bytes 262160 | tf_op jit(solution)/shard_map/reduce_scatter | solution.py:106
  189.7 1.8 convert_element_type.79
  191.9 1.8 fusion.36
  193.6 2.7 %reshape.297 = f32[2048,256]{1,0:T(8,128)} reshape(f32[32,16384]{1,0:T(8,128)} %fusion.36) | data formatting | bytes 4194304 | tf_op jit(solution)/shard_map/reshape | solution.py:129
  (69 shorter events, 20.0 us)
Async XLA Ops:
  7.2 23.6 %copy-start = (bf16[512,2048]{1,0:T(8,128)(2,1)S(1)}, bf16[512,2048]{1,0:T(8,128)(2,1)}, u32[]{:S(2)}) copy-start(bf16[512,2048]{1,0:T(8,128)(2,1)} %param.8) | copy-start | bytes 6291460
  7.2 8.7 %copy-start.2 = (bf16[2048,256]{1,0:T(8,128)(2,1)S(1)}, bf16[2048,256]{1,0:T(8,128)(2,1)}, u32[]{:S(2)}) copy-start(bf16[2048,256]{1,0:T(8,128)(2,1)} %param.14) | copy-start | bytes 3145732
  9.2 24.7 %all-to-all-start = ((s32[4,1,4]{2,1,0:T(1,128)}), s32[4,1,4]{2,1,0:T(1,128)S(1)}, u32[]{:S(2)}, u32[]{:S(2)}) async-start(s32[4,1,4]{2,1,0:T(1,128)} %bitcast), calls=%async_computation | async-start | bytes 4096 | tf_op jit(solution)/shard_map/all_to_all | solution.py:33
  15.9 1.4 copy-start.8
  26.6 4.2 %copy-start.5 = (bf16[2048,256]{1,0:T(8,128)(2,1)S(1)}, bf16[2048,256]{1,0:T(8,128)(2,1)}, u32[]{:S(2)}) copy-start(bf16[2048,256]{1,0:T(8,128)(2,1)} %param.12) | copy-start | bytes 3145732
  30.8 2.8 %copy-start.9 = (bf16[512,256]{1,0:T(8,128)(2,1)S(1)}, bf16[512,256]{1,0:T(8,128)(2,1)}, u32[]{:S(2)}) copy-start(bf16[512,256]{1,0:T(8,128)(2,1)} %param.15) | copy-start | bytes 786436
  40.8 18.0 %all-to-all-start.1 = ((bf16[4,4,64,512]{3,2,1,0:T(8,128)(2,1)}), bf16[4,4,64,512]{3,2,1,0:T(8,128)(2,1)}, u32[]{:S(2)}, u32[]{:S(2)}) async-start(bf16[4,4,64,512]{3,2,1,0:T(8,128)(2,1)} %select_select_fusion), calls=%async_computation.1 | async-start | bytes 2097152 | tf_op jit(solution)/shard_map/all_to_all | solution.py:42
  45.0 75.0 %reduce-scatter.6.cloned.1.call-start = ((), (), s32[]{:S(2)}) async-start(), calls=%async_computation.7 | async-start | bytes 2359296 | tf_op jit(solution)/shard_map/reduce_scatter | solution.py:109
  50.8 14.5 %copy-start.3 = (bf16[4,128,2,128]{1,3,2,0:T(8,128)(2,1)S(1)}, bf16[4,128,2,128]{1,3,2,0:T(8,128)(2,1)}, u32[]{:S(2)}) copy-start(bf16[4,128,2,128]{1,3,2,0:T(8,128)(2,1)} %copy.132) | copy-start | bytes 786436
  64.5 0.8 copy-start.1
  70.7 2.7 %copy-start.10 = (bf16[4,128,1,2,128]{1,4,3,0,2:T(8,128)(2,1)S(1)}, bf16[4,128,1,2,128]{1,4,3,0,2:T(8,128)(2,1)}, u32[]{:S(2)}) copy-start(bf16[4,128,1,2,128]{1,4,3,0,2:T(8,128)(2,1)} %fusion.19) | copy-start | bytes 786436
  83.6 67.1 %reduce-scatter.8.cloned.1.call-start = ((), (), s32[]{:S(2)}) async-start(), calls=%async_computation.8 | async-start | bytes 1310720 | tf_op jit(solution)/shard_map/reduce_scatter | solution.py:89
  89.1 100.6 %reduce-scatter.4.cloned.1.call-start = ((), (), s32[]{:S(2)}) async-start(), calls=%async_computation.6 | async-start | bytes 2359296 | tf_op jit(solution)/shard_map/reduce_scatter | solution.py:106
  91.4 4.5 %copy-start.4 = (bf16[2048,256]{1,0:T(8,128)(2,1)S(1)}, bf16[2048,256]{1,0:T(8,128)(2,1)}, u32[]{:S(2)}) copy-start(bf16[2048,256]{1,0:T(8,128)(2,1)} %param.11) | copy-start | bytes 3145732
  95.9 1.2 copy-start.6
  95.9 1.3 copy-start.7
  122.3 69.1 %all-to-all-start.2 = ((bf16[4,4,64,256]{3,1,2,0:T(4,128)(2,1)}), bf16[4,4,64,256]{3,1,2,0:T(4,128)(2,1)S(1)}, u32[]{:S(2)}, u32[]{:S(2)}) async-start(bf16[4,4,64,256]{3,1,2,0:T(4,128)(2,1)} %convolution_convert_fusion.3), calls=%async_computation.4 | async-start | bytes 1048576 | tf_op jit(solution)/shard_map/all_to_all | solution.py:120
Sparse Core Ops, SparseCore 0:
  83.7 36.3 reduce-scatter.5
  123.0 27.6 reduce-scatter.7
  153.6 36.0 reduce-scatter.3
where the time goes:
time: 204 us; the launch traced here: 203 us
  waiting for transfers between devices  90.6 us (44%)
  matrix products  38.7 us (19%)
  local copies, waits for them, and re-layouts  37.8 us (19%)
  between operations  13.9 us (7%)
  starting transfers between devices  13.3 us (7%)
  other arithmetic  8.45 us (4%)
    reduce_scatter x1, waiting for transfers between devices, shards(): lax.psum_scatter(row_part.astype(jnp.bfloat16), 'tp', scatter_dimension=1...  37.1 us
    reduce_scatter x1, waiting for transfers between devices, shards(): lax.psum_scatter(lax.dot_general(normed, d_query, (((0,), (0,)), ((), ())...  24.7 us
    reduce_scatter x1, waiting for transfers between devices, shards(): lax.psum_scatter(per_request.astype(jnp.bfloat16), 'tp', scatter_dimensio...  20.8 us
    dot_general x1, matrix products, shards(): jnp.dot(store, w_pair, preferred_element_type=jnp.float32)  9.28 us
    all_to_all x1, waiting for transfers between devices, shards(): lax.all_to_all(served.reshape(peer_count, slot_most, PLEN, 2 * head_width...  7.96 us
    unnamed x27, local copies, waits for them, and re-layouts  7.1 us
    all_to_all x1, starting transfers between devices, shards(): lax.all_to_all(slot_table.reshape(peer_count, slot_most), 'st', split_axi...  5.19 us
    gather x2, local copies, waits for them, and re-layouts, shards(): jnp.take(arrived.reshape(slot_count, PLEN, 2 * head_width), slot_of, axis=0)  4.55 us
  transfers between devices with their start and end apart: 6, of which 4 were waited for; matrix products, arithmetic and copies ran while one was open for 22% of the time, Pallas kernels for 0%

commit v1 on v0

v1 whole, which is shorter than its diff:
```python
import functools

import jax
import jax.numpy as jnp
from jax import lax
from jax.experimental import pallas as pl
from jax.experimental.pallas import tpu as pltpu
from jax.sharding import PartitionSpec as P

DH = 128
BLK = 128
PLEN = 64
GROUP = 4
CORES = 2
F32 = jnp.float32
BF16 = jnp.bfloat16
MESH = pl.DeviceIdType.MESH


def dot_nn(a, b):
    return lax.dot_general(a, b, (((1,), (0,)), ((), ())), preferred_element_type=F32)


def dot_nt(a, b):
    return lax.dot_general(a, b, (((1,), (1,)), ((), ())), preferred_element_type=F32)


def dot_tn(a, b):
    return lax.dot_general(a, b, (((0,), (0,)), ((), ())), preferred_element_type=F32)


def rows_at(index, size):
    return pl.ds(pl.multiple_of(index * size, size), size)


def project_kernel(ids, *refs):
    passages = refs[:GROUP]
    wk_ref, wv_ref, out_ref = refs[GROUP:]
    rows = jnp.concatenate([p[...] for p in passages], axis=0)
    width = wk_ref.shape[1]
    out_ref[:, :width] = dot_nn(rows, wk_ref[...]).astype(BF16)
    out_ref[:, width:] = dot_nn(rows, wv_ref[...]).astype(BF16)


def project(store, ids, w_key, w_value):
    slots = ids.shape[0]
    depth, width = w_key.shape
    passage = lambda g: pl.BlockSpec((PLEN, depth), lambda i, ids: (ids[GROUP * i + g], 0))
    weight = pl.BlockSpec((depth, width), lambda i, ids: (0, 0))
    return pl.pallas_call(
        project_kernel,
        out_shape=jax.ShapeDtypeStruct((slots * PLEN, 2 * width), BF16),
        grid_spec=pltpu.PrefetchScalarGridSpec(
            num_scalar_prefetch=1,
            grid=(slots // GROUP,),
            in_specs=[passage(g) for g in range(GROUP)] + [weight, weight],
            out_specs=pl.BlockSpec((GROUP * PLEN, 2 * width), lambda i, ids: (i, 0)),
        ),
        compiler_params=pltpu.CompilerParams(vmem_limit_bytes=32 << 20),
        name="project",
    )(ids, *([store] * GROUP), w_key, w_value)


def main_kernel(
    st_n, tp_n, reads,
    slot_of, req_of, served, normed, w_q, w_g, w_k, w_v, cot,
    rows_out, ret_out, gqw_out,
    arrived, q_s, gate_s, dq_s, dg_s, dp_s,
    x_out, x_in, z_out, z_in, own, part, r_out, r_in, g_out, g_in, g_own,
    kv_ss, kv_rs, x_ss, x_rs, z_ss, z_rs, r_ss, r_rs, g_ss, g_rs,
):
    me_st, me_tp = lax.axis_index("st"), lax.axis_index("tp")
    z_n = tp_n // CORES
    me_z, me_c = me_tp // CORES, me_tp % CORES
    mate = (me_st, me_z * CORES + 1 - me_c)
    tok, hw = cot.shape
    depth = w_q.shape[0]
    heads = hw // DH
    blocks = tok // BLK
    cw = depth // tp_n
    slots = served.shape[0] // st_n
    scale = DH ** (-0.5)

    def st_peer(d):
        return lax.rem(me_st + d, st_n)

    def st_from(d):
        return lax.rem(me_st + st_n - d, st_n)

    def z_peer(d):
        return lax.rem(me_z + d, z_n)

    barrier = pltpu.get_barrier_semaphore()
    for d in range(1, st_n):
        pl.semaphore_signal(barrier, inc=1, device_id=(st_peer(d), me_tp), device_id_type=MESH)
    for d in range(1, z_n):
        pl.semaphore_signal(
            barrier, inc=1, device_id=(me_st, z_peer(d) * CORES + me_c), device_id_type=MESH
        )
    pl.semaphore_signal(barrier, inc=1, device_id=mate, device_id_type=MESH)
    pl.semaphore_wait(barrier, st_n + z_n - 1)

    def remote(src, dst, ss, rs, dev):
        return pltpu.make_async_remote_copy(
            src_ref=src, dst_ref=dst, send_sem=ss, recv_sem=rs, device_id=dev, device_id_type=MESH
        )

    sends = []

    def go(copy):
        copy.start()
        sends.append(copy)

    for d in range(1, st_n):
        go(remote(
            served.at[rows_at(st_peer(d), slots)], arrived.at[rows_at(me_st, slots)],
            kv_ss.at[d], kv_rs.at[d], (st_peer(d), me_tp),
        ))
    arrived[rows_at(me_st, slots)] = served[rows_at(me_st, slots)]

    tile = 2 * BLK

    @pl.loop(0, tok // tile)
    def _(i):
        span = rows_at(i, tile)
        q_s[span, :] = dot_nn(normed[span, :], w_q[...]).astype(BF16)
        gate_s[span, :] = jax.nn.sigmoid(dot_nn(normed[span, :], w_g[...]))

    for d in range(1, st_n):
        here = arrived.at[rows_at(st_from(d), slots)]
        remote(here, here, kv_ss.at[d], kv_rs.at[d], (st_peer(d), me_tp)).wait_recv()

    for b in range(blocks):
        kv = jnp.concatenate(
            [arrived[slot_of[b * reads + r]] for r in range(reads)], axis=0
        )
        toks = slice(b * BLK, (b + 1) * BLK)
        span = reads * PLEN
        ctx = slice(b * span, (b + 1) * span)
        for h in range(heads):
            ch = slice(h * DH, (h + 1) * DH)
            chv = slice(hw + h * DH, hw + (h + 1) * DH)
            k, v = kv[:, ch], kv[:, chv]
            q = q_s[toks, ch]
            gate = gate_s[toks, ch]
            up = cot[toks, ch].astype(F32)
            s = dot_nt(q, k) * scale
            e = jnp.exp(s - jnp.max(s, axis=1, keepdims=True))
            p = e / jnp.sum(e, axis=1, keepdims=True)
            low = p.astype(BF16)
            att = dot_nn(low, v)
            d_att = (up * gate).astype(BF16)
            dg_s[toks, ch] = (up * att * gate * (1.0 - gate)).astype(BF16)
            dp_s[ctx, chv] = dot_tn(low, d_att).astype(BF16)
            d_p = dot_nt(d_att, v)
            delta = jnp.sum(d_p * p, axis=1, keepdims=True)
            d_s = (p * (d_p - delta) * scale).astype(BF16)
            dq_s[toks, ch] = dot_nn(d_s, k).astype(BF16)
            dp_s[ctx, ch] = dot_tn(d_s, q).astype(BF16)

    def chunk(which, t):
        w_rows = rows_at(t, cw)
        if which == 0:
            return dot_nt(dp_s[:, :hw], w_k[w_rows, :]) + dot_nt(dp_s[:, hw:], w_v[w_rows, :])
        return dot_nt(dq_s[...], w_q[w_rows, :]) + dot_nt(dg_s[...], w_g[w_rows, :])

    order = list(range(1, z_n)) + [0]

    def mate_stage(which):
        for d in order:
            n = which * z_n + d
            x_out[n] = chunk(which, z_peer(d) * CORES + 1 - me_c).astype(BF16)
            go(remote(x_out.at[n], x_in.at[n], x_ss.at[n], x_rs.at[n], mate))

    def chip_stage(which):
        for d in order:
            n = which * z_n + d
            mine = chunk(which, z_peer(d) * CORES + me_c)
            remote(x_in.at[n], x_in.at[n], x_ss.at[n], x_rs.at[n], mate).wait_recv()
            total = mine + x_in[n].astype(F32)
            if d == 0:
                own[which] = total
            else:
                z_out[n] = total.astype(BF16)
                go(remote(
                    z_out.at[n], z_in.at[n], z_ss.at[n], z_rs.at[n],
                    (me_st, z_peer(d) * CORES + me_c),
                ))

    def gathered(which):
        total = own[which]
        for d in range(1, z_n):
            n = which * z_n + d
            remote(
                z_in.at[n], z_in.at[n], z_ss.at[n], z_rs.at[n],
                (me_st, z_peer(d) * CORES + me_c),
            ).wait_recv()
            total = total + z_in[n].astype(F32)
        return total

    mate_stage(0)
    chip_stage(0)
    mate_stage(1)
    chip_stage(1)

    dw = depth // st_n
    for d in list(range(1, st_n)) + [0]:
        term = dot_tn(normed[:, rows_at(st_peer(d), dw)], dq_s[...])
        if d == 0:
            g_own[...] = term
        else:
            g_out[d] = term.astype(BF16)
            go(remote(
                g_out.at[d], g_in.at[d], g_ss.at[d], g_rs.at[d], (st_peer(d), me_tp)
            ))

    part[...] = gathered(0).astype(BF16).reshape(part.shape)
    for s in range(st_n * slots):
        r_out[s] = part[req_of[s]]
    for d in range(1, st_n):
        go(remote(
            r_out.at[rows_at(st_peer(d), slots)], r_in.at[rows_at(me_st, slots)],
            r_ss.at[d], r_rs.at[d], (st_peer(d), me_tp),
        ))
    ret_out[rows_at(me_st, slots)] = r_out[rows_at(me_st, slots)]

    total = g_own[...]
    for d in range(1, st_n):
        remote(g_in.at[d], g_in.at[d], g_ss.at[d], g_rs.at[d], (st_peer(d), me_tp)).wait_recv()
        total = total + g_in[d].astype(F32)
    gqw_out[...] = total

    for d in range(1, st_n):
        span = rows_at(st_from(d), slots)
        remote(
            r_in.at[span], r_in.at[span], r_ss.at[d], r_rs.at[d], (st_peer(d), me_tp)
        ).wait_recv()
        ret_out[span] = r_in[span]

    rows_out[...] = gathered(1)
    for copy in sends:
        copy.wait_send()


def main_call(st_n, tp_n, reads, slot_of, req_of, served, normed, w_q, w_g, w_k, w_v, cot):
    tok, hw = cot.shape
    depth = w_q.shape[0]
    cw, dw, z_n = depth // tp_n, depth // st_n, tp_n // CORES
    ctx = tok // BLK * reads * PLEN
    slot_total = served.shape[0]
    vmem = pl.BlockSpec(memory_space=pltpu.VMEM)
    smem = pl.BlockSpec(memory_space=pltpu.SMEM)
    piece = lambda rows, n=2 * z_n: pltpu.VMEM((n, rows, cw), BF16)
    sem = lambda n: pltpu.SemaphoreType.DMA((n,))
    rows_most = max(ctx, tok)
    assert ctx == tok
    return pl.pallas_call(
        functools.partial(main_kernel, st_n, tp_n, reads),
        out_shape=(
            jax.ShapeDtypeStruct((tok, cw), F32),
            jax.ShapeDtypeStruct((slot_total, PLEN, cw), BF16),
            jax.ShapeDtypeStruct((dw, hw), F32),
        ),
        in_specs=[smem, smem] + [vmem] * 7,
        out_specs=(vmem, vmem, vmem),
        scratch_shapes=[
            pltpu.VMEM((slot_total, PLEN, 2 * hw), BF16),
            pltpu.VMEM((tok, hw), BF16),
            pltpu.VMEM((tok, hw), F32),
            pltpu.VMEM((tok, hw), BF16),
            pltpu.VMEM((tok, hw), BF16),
            pltpu.VMEM((ctx, 2 * hw), BF16),
            piece(rows_most), piece(rows_most), piece(rows_most), piece(rows_most),
            pltpu.VMEM((2, rows_most, cw), F32),
            pltpu.VMEM((ctx // PLEN, PLEN, cw), BF16),
            pltpu.VMEM((slot_total, PLEN, cw), BF16),
            pltpu.VMEM((slot_total, PLEN, cw), BF16),
            pltpu.VMEM((st_n, dw, hw), BF16),
            pltpu.VMEM((st_n, dw, hw), BF16),
            pltpu.VMEM((dw, hw), F32),
            sem(st_n), sem(st_n), sem(2 * z_n), sem(2 * z_n), sem(2 * z_n), sem(2 * z_n),
            sem(st_n), sem(st_n), sem(st_n), sem(st_n),
        ],
        compiler_params=pltpu.CompilerParams(
            collective_id=0, has_side_effects=True, vmem_limit_bytes=56 << 20
        ),
        name="main",
    )(slot_of, req_of, served, normed, w_q, w_g, w_k, w_v, cot)


def spread_kernel(ids, returned, out_ref):
    out_ref[...] = jnp.zeros_like(out_ref)
    for s in range(ids.shape[0]):
        passage = ids[s]

        @pl.when(passage >= 0)
        def _():
            span = rows_at(passage, PLEN)
            out_ref[span, :] += returned[s].astype(F32)


def spread(ids, returned, rows):
    return pl.pallas_call(
        spread_kernel,
        out_shape=jax.ShapeDtypeStruct((rows, returned.shape[2]), F32),
        in_specs=[
            pl.BlockSpec(memory_space=pltpu.SMEM),
            pl.BlockSpec(memory_space=pltpu.VMEM),
        ],
        out_specs=pl.BlockSpec(memory_space=pltpu.VMEM),
        compiler_params=pltpu.CompilerParams(vmem_limit_bytes=16 << 20),
        name="spread",
    )(ids, returned)


def shards(normed, store, passage_ids, w_query, w_gate, w_key, w_value, cotangent):
    peer_count = lax.axis_size("st")
    blocks, read_count = passage_ids.shape
    requests = blocks * read_count
    slot_most = max(1, 2 * requests // peer_count)
    slot_count = peer_count * slot_most
    pass_dev = store.shape[0] // PLEN
    flat_ids = passage_ids.reshape(requests)
    owners = flat_ids // pass_dev
    local_ids = flat_ids % pass_dev
    positions = jnp.arange(requests, dtype=jnp.int32)
    before = (owners[:, None] == owners[None, :]) & (positions[None, :] < positions[:, None])
    slot_of = owners * slot_most + jnp.sum(before.astype(jnp.int32), axis=1)
    slot_hit = slot_of[:, None] == jnp.arange(slot_count, dtype=jnp.int32)[None, :]
    slot_table = jnp.max(jnp.where(slot_hit, local_ids[:, None], -1), axis=0)
    req_of = jnp.max(jnp.where(slot_hit, positions[:, None], 0), axis=0)
    served_ids = lax.all_to_all(
        slot_table.reshape(peer_count, slot_most), "st", split_axis=0, concat_axis=0, tiled=True
    ).reshape(slot_count)
    served = project(store, jnp.maximum(served_ids, 0), w_key, w_value)
    served = served.reshape(slot_count, PLEN, served.shape[1])
    grad_rows, returned, grad_query_weight = main_call(
        peer_count, lax.axis_size("tp"), read_count,
        slot_of, req_of, served, normed, w_query, w_gate, w_key, w_value, cotangent,
    )
    grad_store = spread(served_ids, returned, store.shape[0])
    return (grad_rows, grad_store, grad_query_weight)


def solution(mesh):
    placed = (
        P("st", None),
        P("st", None),
        P("st", None),
        P(None, "tp"),
        P(None, "tp"),
        P(None, "tp"),
        P(None, "tp"),
        P("st", "tp"),
    )
    return jax.shard_map(
        shards,
        mesh=mesh,
        in_specs=placed,
        out_specs=(P("st", "tp"), P("st", "tp"), P("st", "tp")),
        check_vma=False,
    )
```

time: 204 us -> 96.8 us (0.47)
  the two profiles are of different devices: /device:TPU:0 before, /device:TPU:8 now
where the time goes in v1:
time: 96.8 us; the launch traced here: 96.5 us
  Pallas kernels  75.2 us (78%)
  local copies, waits for them, and re-layouts  11 us (11%)
  blocking collectives  8.18 us (8%)
  other arithmetic  1.47 us (2%)
    pallas_call x1, Pallas kernels, main_call(): pl.pallas_call(functools.partial(main_kernel, st_n, tp_n, reads), out_sha...  69.6 us
    unnamed x19, local copies, waits for them, and re-layouts  10.2 us
    all_to_all x1, blocking collectives, shards(): lax.all_to_all(slot_table.reshape(peer_count, slot_most), 'st', split_axi...  8.18 us
    pallas_call x1, Pallas kernels, project(): pl.pallas_call(project_kernel, out_shape=jax.ShapeDtypeStruct((slots * PL...  3.41 us
    pallas_call x1, Pallas kernels, spread(): pl.pallas_call(spread_kernel, out_shape=jax.ShapeDtypeStruct((rows, retur...  2.14 us

profile of v1, /device:TPU:8, one launch (start us, length us, event | category | flops | bytes accessed | tf_op | source)
XLA Modules:
  0.0 96.5 jit_solution(11488459795273702509)
XLA Ops:
  0.6 0.8 copy.15
  1.4 0.1 reshape.110
  1.5 0.2 convert_reduce_fusion
  1.7 0.0 copy-start.7
  1.7 0.6 select_reduce_fusion
  2.3 0.1 all_to_all.6
  2.4 8.2 %all_to_all.9 = s32[4,1,4]{2,1,0:T(1,128)S(1)} all-to-all(s32[4,1,4]{2,1,0:T(1,128)S(1)} %bitcast.3), channel_id=1, replica_groups=mesh['st'=4,'tp'=8] {'st'}, dimensions={0} | all-to-all | bytes 128 | tf_op jit(solution)/shard_map/all_to_all | solution.py:332
  10.6 0.5 broadcast.133
  11.1 0.7 reduce.3
  11.7 0.1 reshape.111.ids
  11.8 0.0 copy-start
  11.8 3.4 %copy-done = bf16[2048,2048]{1,0:T(8,128)(2,1)S(1)} copy-done((bf16[2048,2048]{1,0:T(8,128)(2,1)S(1)}, bf16[2048,2048]{1,0:T(8,128)(2,1)}, u32[]{:S(2)}) %copy-start) | copy-done | bytes 8388632
  15.2 0.0 copy-start.1
  15.2 1.2 %copy-done.1 = bf16[2048,256]{1,0:T(8,128)(2,1)S(1)} copy-done((bf16[2048,256]{1,0:T(8,128)(2,1)S(1)}, bf16[2048,256]{1,0:T(8,128)(2,1)}, u32[]{:S(2)}) %copy-start.1) | copy-done | bytes 1048600
  16.4 0.0 copy-start.2
  16.4 1.2 %copy-done.2 = bf16[2048,256]{1,0:T(8,128)(2,1)S(1)} copy-done((bf16[2048,256]{1,0:T(8,128)(2,1)S(1)}, bf16[2048,256]{1,0:T(8,128)(2,1)}, u32[]{:S(2)}) %copy-start.2) | copy-done | bytes 1048600
  17.7 3.4 %project.1 = bf16[1024,512]{1,0:T(8,128)(2,1)S(1)} custom-call(s32[16]{0:T(128)S(1)} %broadcast_maximum_fusion.ids, bf16[2048,2048]{1,0:T(8,128)(2,1)S(1)} %copy-done, bf16[2048,2048]{1,0:T(8,128)(2,1)S(1)} %copy-done, bf16[2048,2048]{1,0:T(8,128)(2,1)S(1)} %copy-done, bf16[2048,2048]{1,0:T(8,128)(2,1)S(1)} %copy-done, bf16[2048,256]{1,0:T(8,128)(2,1)S(1)} %copy-done.1, ...), custom_call_target="tpu_custom_call" | custom-call | tf_op jit(solution)/shard_map/project/pallas_call | solution.py:50
  21.1 0.0 copy-done.7
  21.1 0.0 copy-start.3
  21.1 1.0 copy-done.3
  22.1 69.6 %main.1 = (f32[512,256]{1,0:T(8,128)}, bf16[16,64,256]{2,1,0:T(8,128)(2,1)}, f32[512,256]{1,0:T(8,128)}) custom-call(s32[8]{0:T(128)} %copy-done.7, s32[16]{0:T(128)} %get-tuple-element.10.req_of, bf16[16,64,512]{2,1,0:T(8,128)(2,1)} %bitcast.2, bf16[512,2048]{1,0:T(8,128)(2,1)} %normed.1, bf16[2048,256]{1,0:T(8,128)(2,1)} %w_q.1, bf16[2048,256]{1,0:T(8,128)(2,1)} %w_g.1, ...), custom_call_target="tpu_custom_call" | custom-call | tf_op jit(solution)/shard_map/main/pallas_call | solution.py:257
  91.7 0.0 copy-start.4
  91.7 1.0 %copy-done.4 = bf16[16,64,256]{2,1,0:T(8,128)(2,1)S(1)} copy-done((bf16[16,64,256]{2,1,0:T(8,128)(2,1)S(1)}, bf16[16,64,256]{2,1,0:T(8,128)(2,1)}, u32[]{:S(2)}) %copy-start.4) | copy-done | bytes 524312
  92.7 0.0 copy-start.6
  92.7 0.0 copy-start.5
  92.7 2.1 %spread.1 = f32[2048,256]{1,0:T(8,128)} custom-call(s32[16]{0:T(128)S(1)} %reshape.111.ids, bf16[16,64,256]{2,1,0:T(8,128)(2,1)S(1)} %copy-done.4), custom_call_target="tpu_custom_call" | custom-call | tf_op jit(solution)/shard_map/spread/pallas_call | solution.py:303
  94.9 0.0 copy-done.6
  94.9 0.8 copy.19
  95.7 0.0 copy-done.5
  95.7 0.8 copy.20
  (3 shorter events, 0.0 us)
Async XLA Ops:
  1.7 19.4 %copy-start.7 = (s32[8]{0:T(128)}, s32[8]{0:T(128)S(1)}, u32[]{:S(2)}) copy-start(s32[8]{0:T(128)S(1)} %multiply_add_fusion.slot_of) | copy-start | bytes 100
  11.8 3.4 %copy-start = (bf16[2048,2048]{1,0:T(8,128)(2,1)S(1)}, bf16[2048,2048]{1,0:T(8,128)(2,1)}, u32[]{:S(2)}) copy-start(bf16[2048,2048]{1,0:T(8,128)(2,1)} %refs_3_.1) | copy-start | bytes 25165828
  15.2 1.2 %copy-start.1 = (bf16[2048,256]{1,0:T(8,128)(2,1)S(1)}, bf16[2048,256]{1,0:T(8,128)(2,1)}, u32[]{:S(2)}) copy-start(bf16[2048,256]{1,0:T(8,128)(2,1)} %w_k.1) | copy-start | bytes 3145732
  16.4 1.2 %copy-start.2 = (bf16[2048,256]{1,0:T(8,128)(2,1)S(1)}, bf16[2048,256]{1,0:T(8,128)(2,1)}, u32[]{:S(2)}) copy-start(bf16[2048,256]{1,0:T(8,128)(2,1)} %w_v.1) | copy-start | bytes 3145732
  21.1 1.0 %copy-start.3 = (bf16[1024,512]{1,0:T(8,128)(2,1)}, bf16[1024,512]{1,0:T(8,128)(2,1)S(1)}, u32[]{:S(2)}) copy-start(bf16[1024,512]{1,0:T(8,128)(2,1)S(1)} %project.1) | copy-start | bytes 3145732
  91.7 1.0 %copy-start.4 = (bf16[16,64,256]{2,1,0:T(8,128)(2,1)S(1)}, bf16[16,64,256]{2,1,0:T(8,128)(2,1)}, u32[]{:S(2)}) copy-start(bf16[16,64,256]{2,1,0:T(8,128)(2,1)} %get-tuple-element.7.returned) | copy-start | bytes 1572868
  92.7 2.1 %copy-start.6 = (f32[512,256]{1,0:T(8,128)S(1)}, f32[512,256]{1,0:T(8,128)}, u32[]{:S(2)}) copy-start(f32[512,256]{1,0:T(8,128)} %get-tuple-element.16) | copy-start | bytes 1572868
  92.7 2.9 %copy-start.5 = (f32[512,256]{1,0:T(8,128)S(1)}, f32[512,256]{1,0:T(8,128)}, u32[]{:S(2)}) copy-start(f32[512,256]{1,0:T(8,128)} %get-tuple-element.18) | copy-start | bytes 1572868

commit v2 on v1

--- a/solution.py
+++ b/solution.py
@@ -56,7 +56,7 @@
             in_specs=[passage(g) for g in range(GROUP)] + [weight, weight],
             out_specs=pl.BlockSpec((GROUP * PLEN, 2 * width), lambda i, ids: (i, 0)),
         ),
-        compiler_params=pltpu.CompilerParams(vmem_limit_bytes=32 << 20),
+        compiler_params=pltpu.CompilerParams(vmem_limit_bytes=58 << 20),
         name="project",
     )(ids, *([store] * GROUP), w_key, w_value)
 
@@ -66,8 +66,8 @@
     slot_of, req_of, served, normed, w_q, w_g, w_k, w_v, cot,
     rows_out, ret_out, gqw_out,
     arrived, q_s, gate_s, dq_s, dg_s, dp_s,
-    x_out, x_in, z_out, z_in, own, part, r_out, r_in, g_out, g_in, g_own,
-    kv_ss, kv_rs, x_ss, x_rs, z_ss, z_rs, r_ss, r_rs, g_ss, g_rs,
+    x_out, x_in, z_out, up_in, dn_in, own, part, r_out, r_in, g_out, g_in, g_own,
+    kv_ss, kv_rs, x_ss, x_rs, z_ss, up_rs, dn_rs, r_ss, r_rs, g_ss, g_rs,
 ):
     me_st, me_tp = lax.axis_index("st"), lax.axis_index("tp")
     z_n = tp_n // CORES
@@ -164,39 +164,80 @@
             return dot_nt(dp_s[:, :hw], w_k[w_rows, :]) + dot_nt(dp_s[:, hw:], w_v[w_rows, :])
         return dot_nt(dq_s[...], w_q[w_rows, :]) + dot_nt(dg_s[...], w_g[w_rows, :])
 
-    order = list(range(1, z_n)) + [0]
+    order = []
+    for i in range((z_n + 1) // 2):
+        order += [z_n - 1 - i, i] if z_n - 1 - i != i else [i]
+    above, below = me_z < z_n - 1, me_z > 0
 
     def mate_stage(which):
-        for d in order:
-            n = which * z_n + d
-            x_out[n] = chunk(which, z_peer(d) * CORES + 1 - me_c).astype(BF16)
+        for t in order:
+            n = which * z_n + t
+            x_out[n] = chunk(which, t * CORES + 1 - me_c).astype(BF16)
             go(remote(x_out.at[n], x_in.at[n], x_ss.at[n], x_rs.at[n], mate))
 
+    def hop(n, up):
+        landing, rs = (up_in, up_rs) if up else (dn_in, dn_rs)
+        to = me_z + 1 if up else me_z - 1
+        return remote(
+            z_out.at[n], landing.at[n], z_ss.at[n], rs.at[n], (me_st, to * CORES + me_c)
+        )
+
     def chip_stage(which):
-        for d in order:
-            n = which * z_n + d
-            mine = chunk(which, z_peer(d) * CORES + me_c)
+        for t in order:
+            n = which * z_n + t
+            mine = chunk(which, t * CORES + me_c)
             remote(x_in.at[n], x_in.at[n], x_ss.at[n], x_rs.at[n], mate).wait_recv()
             total = mine + x_in[n].astype(F32)
-            if d == 0:
-                own[which] = total
-            else:
+            own[n] = total
+
+            @pl.when(jnp.logical_and(me_z == 0, t > me_z))
+            def _():
                 z_out[n] = total.astype(BF16)
-                go(remote(
-                    z_out.at[n], z_in.at[n], z_ss.at[n], z_rs.at[n],
-                    (me_st, z_peer(d) * CORES + me_c),
-                ))
-
-    def gathered(which):
-        total = own[which]
-        for d in range(1, z_n):
-            n = which * z_n + d
-            remote(
-                z_in.at[n], z_in.at[n], z_ss.at[n], z_rs.at[n],
-                (me_st, z_peer(d) * CORES + me_c),
-            ).wait_recv()
-            total = total + z_in[n].astype(F32)
-        return total
+                hop(n, True).start()
+
+            @pl.when(jnp.logical_and(me_z == z_n - 1, t < me_z))
+            def _():
+                z_out[n] = total.astype(BF16)
+                hop(n, False).start()
+
+    def relay_stage(which):
+        for t in order:
+            n = which * z_n + t
+
+            @pl.when(jnp.logical_and(below, t > me_z))
+            def _():
+                hop(n, True).wait_recv()
+                z_out[n] = (own[n] + up_in[n].astype(F32)).astype(BF16)
+                hop(n, True).start()
+
+            @pl.when(jnp.logical_and(above, t < me_z))
+            def _():
+                hop(n, False).wait_recv()
+                z_out[n] = (own[n] + dn_in[n].astype(F32)).astype(BF16)
+                hop(n, False).start()
+
+    def gathered(which, put):
+        for t in range(z_n):
+            n = which * z_n + t
+
+            @pl.when(t == me_z)
+            def _():
+                if t > 0:
+                    hop(n, True).wait_recv()
+                if t < z_n - 1:
+                    hop(n, False).wait_recv()
+                total = own[n]
+                if t > 0:
+                    total = total + up_in[n].astype(F32)
+                if t < z_n - 1:
+                    total = total + dn_in[n].astype(F32)
+                put(total)
+
+    def put_part(total):
+        part[...] = total.astype(BF16).reshape(part.shape)
+
+    def put_rows(total):
+        rows_out[...] = total
 
     mate_stage(0)
     chip_stage(0)
@@ -214,7 +255,8 @@
                 g_out.at[d], g_in.at[d], g_ss.at[d], g_rs.at[d], (st_peer(d), me_tp)
             ))
 
-    part[...] = gathered(0).astype(BF16).reshape(part.shape)
+    relay_stage(0)
+    gathered(0, put_part)
     for s in range(st_n * slots):
         r_out[s] = part[req_of[s]]
     for d in range(1, st_n):
@@ -224,6 +266,7 @@
         ))
     ret_out[rows_at(me_st, slots)] = r_out[rows_at(me_st, slots)]
 
+    relay_stage(1)
     total = g_own[...]
     for d in range(1, st_n):
         remote(g_in.at[d], g_in.at[d], g_ss.at[d], g_rs.at[d], (st_peer(d), me_tp)).wait_recv()
@@ -237,9 +280,15 @@
         ).wait_recv()
         ret_out[span] = r_in[span]
 
-    rows_out[...] = gathered(1)
+    gathered(1, put_rows)
     for copy in sends:
         copy.wait_send()
+    for t in range(z_n):
+        for which in range(2):
+
+            @pl.when(t != me_z)
+            def _():
+                hop(which * z_n + t, True).wait_send()
 
 
 def main_call(st_n, tp_n, reads, slot_of, req_of, served, normed, w_q, w_g, w_k, w_v, cot):
@@ -270,15 +319,15 @@
             pltpu.VMEM((tok, hw), BF16),
             pltpu.VMEM((tok, hw), BF16),
             pltpu.VMEM((ctx, 2 * hw), BF16),
-            piece(rows_most), piece(rows_most), piece(rows_most), piece(rows_most),
-            pltpu.VMEM((2, rows_most, cw), F32),
+            piece(rows_most), piece(rows_most), piece(rows_most), piece(rows_most), piece(rows_most),
+            pltpu.VMEM((2 * z_n, rows_most, cw), F32),
             pltpu.VMEM((ctx // PLEN, PLEN, cw), BF16),
             pltpu.VMEM((slot_total, PLEN, cw), BF16),
             pltpu.VMEM((slot_total, PLEN, cw), BF16),
             pltpu.VMEM((st_n, dw, hw), BF16),
             pltpu.VMEM((st_n, dw, hw), BF16),
             pltpu.VMEM((dw, hw), F32),
-            sem(st_n), sem(st_n), sem(2 * z_n), sem(2 * z_n), sem(2 * z_n), sem(2 * z_n),
+            sem(st_n), sem(st_n), sem(2 * z_n), sem(2 * z_n), sem(2 * z_n), sem(2 * z_n), sem(2 * z_n),
             sem(st_n), sem(st_n), sem(st_n), sem(st_n),
         ],
         compiler_params=pltpu.CompilerParams(

time: 96.8 us -> 91.5 us (0.945)
  the two profiles are of different devices: /device:TPU:8 before, /device:TPU:0 now
where the time goes in v2:
time: 91.5 us; the launch traced here: 91 us
  Pallas kernels  74.5 us (81%)
  blocking collectives  9.66 us (11%)
  local copies, waits for them, and re-layouts  4.16 us (5%)
  other arithmetic  2.06 us (2%)
    pallas_call x1, Pallas kernels, main_call(): pl.pallas_call(functools.partial(main_kernel, st_n, tp_n, reads), out_sha...  65.6 us
    all_to_all x1, blocking collectives, shards(): lax.all_to_all(slot_table.reshape(peer_count, slot_most), 'st', split_axi...  9.66 us
    pallas_call x1, Pallas kernels, project(): pl.pallas_call(project_kernel, out_shape=jax.ShapeDtypeStruct((slots * PL...  6.77 us
    unnamed x11, local copies, waits for them, and re-layouts  3.4 us
    pallas_call x1, Pallas kernels, spread(): pl.pallas_call(spread_kernel, out_shape=jax.ShapeDtypeStruct((rows, retur...  2.14 us

profile of v2, /device:TPU:0, one launch (start us, length us, event | category | flops | bytes accessed | tf_op | source)
XLA Modules:
  0.0 91.0 jit_solution(9984590032051324029)
XLA Ops:
  0.6 0.8 copy.15
  1.4 0.1 reshape.110
  1.5 0.2 convert_reduce_fusion
  1.7 0.0 copy-start.3
  1.7 0.6 select_reduce_fusion
  2.3 0.1 all_to_all.6
  2.4 9.7 %all_to_all.9 = s32[4,1,4]{2,1,0:T(1,128)S(1)} all-to-all(s32[4,1,4]{2,1,0:T(1,128)S(1)} %bitcast.3), channel_id=1, replica_groups=mesh['st'=4,'tp'=8] {'st'}, dimensions={0} | all-to-all | bytes 128 | tf_op jit(solution)/shard_map/all_to_all | solution.py:381
  12.0 0.5 broadcast.133
  12.5 0.7 reduce.3
  13.2 0.1 reshape.111.ids
  13.3 0.6 broadcast_maximum_fusion.ids
  13.9 6.8 %project.1 = bf16[1024,512]{1,0:T(8,128)(2,1)} custom-call(s32[16]{0:T(128)} %broadcast_maximum_fusion.ids, bf16[2048,2048]{1,0:T(8,128)(2,1)} %refs_3_.1, bf16[2048,2048]{1,0:T(8,128)(2,1)} %refs_3_.1, bf16[2048,2048]{1,0:T(8,128)(2,1)} %refs_3_.1, bf16[2048,2048]{1,0:T(8,128)(2,1)} %refs_3_.1, bf16[2048,256]{1,0:T(8,128)(2,1)} %w_k.1, bf16[2048,256]{1,0:T(8,128)(2,1)} %w_v.1), custom_call_target="tpu_custom_call" | custom-call | tf_op jit(solution)/shard_map/project/pallas_call | solution.py:50
  20.7 0.0 copy-done.3
  20.7 65.6 %main.1 = (f32[512,256]{1,0:T(8,128)}, bf16[16,64,256]{2,1,0:T(8,128)(2,1)}, f32[512,256]{1,0:T(8,128)}) custom-call(s32[8]{0:T(128)} %copy-done.3, s32[16]{0:T(128)} %get-tuple-element.10.req_of, bf16[16,64,512]{2,1,0:T(8,128)(2,1)} %bitcast.2, bf16[512,2048]{1,0:T(8,128)(2,1)} %normed.1, bf16[2048,256]{1,0:T(8,128)(2,1)} %w_q.1, bf16[2048,256]{1,0:T(8,128)(2,1)} %w_g.1, ...), custom_call_target="tpu_custom_call" | custom-call | tf_op jit(solution)/shard_map/main/pallas_call | solution.py:306
  86.2 0.0 copy-start
  86.3 1.0 %copy-done = bf16[16,64,256]{2,1,0:T(8,128)(2,1)S(1)} copy-done((bf16[16,64,256]{2,1,0:T(8,128)(2,1)S(1)}, bf16[16,64,256]{2,1,0:T(8,128)(2,1)}, u32[]{:S(2)}) %copy-start) | copy-done | bytes 524312
  87.3 0.0 copy-start.2
  87.3 0.0 copy-start.1
  87.3 2.1 %spread.1 = f32[2048,256]{1,0:T(8,128)} custom-call(s32[16]{0:T(128)S(1)} %reshape.111.ids, bf16[16,64,256]{2,1,0:T(8,128)(2,1)S(1)} %copy-done), custom_call_target="tpu_custom_call" | custom-call | tf_op jit(solution)/shard_map/spread/pallas_call | solution.py:352
  89.4 0.0 copy-done.2
  89.4 0.8 copy.19
  90.2 0.0 copy-done.1
  90.2 0.8 copy.20
  (2 shorter events, 0.0 us)
Async XLA Ops:
  1.7 19.0 %copy-start.3 = (s32[8]{0:T(128)}, s32[8]{0:T(128)S(1)}, u32[]{:S(2)}) copy-start(s32[8]{0:T(128)S(1)} %multiply_add_fusion.slot_of) | copy-start | bytes 100
  86.2 1.0 %copy-start = (bf16[16,64,256]{2,1,0:T(8,128)(2,1)S(1)}, bf16[16,64,256]{2,1,0:T(8,128)(2,1)}, u32[]{:S(2)}) copy-start(bf16[16,64,256]{2,1,0:T(8,128)(2,1)} %get-tuple-element.7.returned) | copy-start | bytes 1572868
  87.3 2.1 %copy-start.2 = (f32[512,256]{1,0:T(8,128)S(1)}, f32[512,256]{1,0:T(8,128)}, u32[]{:S(2)}) copy-start(f32[512,256]{1,0:T(8,128)} %get-tuple-element.16) | copy-start | bytes 1572868
  87.3 2.9 %copy-start.1 = (f32[512,256]{1,0:T(8,128)S(1)}, f32[512,256]{1,0:T(8,128)}, u32[]{:S(2)}) copy-start(f32[512,256]{1,0:T(8,128)} %get-tuple-element.18) | copy-start | bytes 1572868

commit v3 on v2

--- a/solution.py
+++ b/solution.py
@@ -63,8 +63,9 @@
 
 def main_kernel(
     st_n, tp_n, reads,
-    slot_of, req_of, served, normed, w_q, w_g, w_k, w_v, cot,
+    slot_of, req_of, served, normed_h, w_q_h, w_g_h, w_k_h, w_v_h, cot_h,
     rows_out, ret_out, gqw_out,
+    normed, w_q, w_g, w_k, w_v, cot, load_sem,
     arrived, q_s, gate_s, dq_s, dg_s, dp_s,
     x_out, x_in, z_out, up_in, dn_in, own, part, r_out, r_in, g_out, g_in, g_own,
     kv_ss, kv_rs, x_ss, x_rs, z_ss, up_rs, dn_rs, r_ss, r_rs, g_ss, g_rs,
@@ -90,6 +91,12 @@
     def z_peer(d):
         return lax.rem(me_z + d, z_n)
 
+    loads = []
+    pairs = ((normed_h, normed), (w_q_h, w_q), (w_g_h, w_g), (cot_h, cot), (w_k_h, w_k), (w_v_h, w_v))
+    for i, (far, near) in enumerate(pairs):
+        loads.append(pltpu.make_async_copy(far, near, load_sem.at[i]))
+        loads[-1].start()
+
     barrier = pltpu.get_barrier_semaphore()
     for d in range(1, st_n):
         pl.semaphore_signal(barrier, inc=1, device_id=(st_peer(d), me_tp), device_id_type=MESH)
@@ -118,6 +125,8 @@
         ))
     arrived[rows_at(me_st, slots)] = served[rows_at(me_st, slots)]
 
+    for load in loads:
+        load.wait()
     tile = 2 * BLK
 
     @pl.loop(0, tok // tile)
@@ -169,11 +178,10 @@
         order += [z_n - 1 - i, i] if z_n - 1 - i != i else [i]
     above, below = me_z < z_n - 1, me_z > 0
 
-    def mate_stage(which):
-        for t in order:
-            n = which * z_n + t
-            x_out[n] = chunk(which, t * CORES + 1 - me_c).astype(BF16)
-            go(remote(x_out.at[n], x_in.at[n], x_ss.at[n], x_rs.at[n], mate))
+    def mate_stage(which, t):
+        n = which * z_n + t
+        x_out[n] = chunk(which, t * CORES + 1 - me_c).astype(BF16)
+        go(remote(x_out.at[n], x_in.at[n], x_ss.at[n], x_rs.at[n], mate))
 
     def hop(n, up):
         landing, rs = (up_in, up_rs) if up else (dn_in, dn_rs)
@@ -182,8 +190,8 @@
             z_out.at[n], landing.at[n], z_ss.at[n], rs.at[n], (me_st, to * CORES + me_c)
         )
 
-    def chip_stage(which):
-        for t in order:
+    def chip_stage(which, t):
+        if True:
             n = which * z_n + t
             mine = chunk(which, t * CORES + me_c)
             remote(x_in.at[n], x_in.at[n], x_ss.at[n], x_rs.at[n], mate).wait_recv()
@@ -239,10 +247,13 @@
     def put_rows(total):
         rows_out[...] = total
 
-    mate_stage(0)
-    chip_stage(0)
-    mate_stage(1)
-    chip_stage(1)
+    ahead = 2
+    queue = [(which, t) for which in range(2) for t in order]
+    for i in range(len(queue) + ahead):
+        if i < len(queue):
+            mate_stage(*queue[i])
+        if i >= ahead:
+            chip_stage(*queue[i - ahead])
 
     dw = depth // st_n
     for d in list(range(1, st_n)) + [0]:
@@ -310,9 +321,11 @@
             jax.ShapeDtypeStruct((slot_total, PLEN, cw), BF16),
             jax.ShapeDtypeStruct((dw, hw), F32),
         ),
-        in_specs=[smem, smem] + [vmem] * 7,
+        in_specs=[smem, smem, vmem] + [pl.BlockSpec(memory_space=pl.ANY)] * 6,
         out_specs=(vmem, vmem, vmem),
         scratch_shapes=[
+            *[pltpu.VMEM(a.shape, a.dtype) for a in (normed, w_q, w_g, w_k, w_v, cot)],
+            sem(6),
             pltpu.VMEM((slot_total, PLEN, 2 * hw), BF16),
             pltpu.VMEM((tok, hw), BF16),
             pltpu.VMEM((tok, hw), F32),
@@ -337,7 +350,9 @@
     )(slot_of, req_of, served, normed, w_q, w_g, w_k, w_v, cot)
 
 
-def spread_kernel(ids, returned, out_ref):
+def spread_kernel(ids, returned, rows, gqw, out_ref, rows_ref, gqw_ref):
+    rows_ref[...] = rows[...]
+    gqw_ref[...] = gqw[...]
     out_ref[...] = jnp.zeros_like(out_ref)
     for s in range(ids.shape[0]):
         passage = ids[s]
@@ -348,18 +363,20 @@
             out_ref[span, :] += returned[s].astype(F32)
 
 
-def spread(ids, returned, rows):
+def spread(ids, returned, grad_rows, grad_query_weight, rows):
+    vmem = pl.BlockSpec(memory_space=pltpu.VMEM)
     return pl.pallas_call(
         spread_kernel,
-        out_shape=jax.ShapeDtypeStruct((rows, returned.shape[2]), F32),
-        in_specs=[
-            pl.BlockSpec(memory_space=pltpu.SMEM),
-            pl.BlockSpec(memory_space=pltpu.VMEM),
-        ],
-        out_specs=pl.BlockSpec(memory_space=pltpu.VMEM),
-        compiler_params=pltpu.CompilerParams(vmem_limit_bytes=16 << 20),
+        out_shape=(
+            jax.ShapeDtypeStruct((rows, returned.shape[2]), F32),
+            jax.ShapeDtypeStruct(grad_rows.shape, F32),
+            jax.ShapeDtypeStruct(grad_query_weight.shape, F32),
+        ),
+        in_specs=[pl.BlockSpec(memory_space=pltpu.SMEM), vmem, vmem, vmem],
+        out_specs=(vmem, vmem, vmem),
+        compiler_params=pltpu.CompilerParams(vmem_limit_bytes=60 << 20),
         name="spread",
-    )(ids, returned)
+    )(ids, returned, grad_rows, grad_query_weight)
 
 
 def shards(normed, store, passage_ids, w_query, w_gate, w_key, w_value, cotangent):
@@ -387,7 +404,9 @@
         peer_count, lax.axis_size("tp"), read_count,
         slot_of, req_of, served, normed, w_query, w_gate, w_key, w_value, cotangent,
     )
-    grad_store = spread(served_ids, returned, store.shape[0])
+    grad_store, grad_rows, grad_query_weight = spread(
+        served_ids, returned, grad_rows, grad_query_weight, store.shape[0]
+    )
     return (grad_rows, grad_store, grad_query_weight)
 
 

time: 91.5 us -> 89.9 us (0.983)
  local copies, waits for them, and re-layouts: 4.16 us -> 1.54 us
  Pallas kernels: 74.5 us -> 75.8 us
    unnamed x11 -> x5, local copies, waits for them, and re-layouts: 3.4 us -> 0.77 us
    pallas_call x1, Pallas kernels: 2.14 us -> 3.38 us  [spread(): pl.pallas_call(spread_kernel, out_shape=(jax.ShapeDtypeStruct((rows, retu...]
where the time goes in v3:
time: 89.9 us; the launch traced here: 89.7 us
  Pallas kernels  75.8 us (84%)
  blocking collectives  9.66 us (11%)
  other arithmetic  1.98 us (2%)
  local copies, waits for them, and re-layouts  1.54 us (2%)
    pallas_call x1, Pallas kernels, main_call(): pl.pallas_call(functools.partial(main_kernel, st_n, tp_n, reads), out_sha...  65.6 us
    all_to_all x1, blocking collectives, shards(): lax.all_to_all(slot_table.reshape(peer_count, slot_most), 'st', split_axi...  9.66 us
    pallas_call x1, Pallas kernels, project(): pl.pallas_call(project_kernel, out_shape=jax.ShapeDtypeStruct((slots * PL...  6.84 us
    pallas_call x1, Pallas kernels, spread(): pl.pallas_call(spread_kernel, out_shape=(jax.ShapeDtypeStruct((rows, retu...  3.38 us

profile of v3, /device:TPU:0, one launch (start us, length us, event | category | flops | bytes accessed | tf_op | source)
XLA Modules:
  0.0 89.7 jit_solution(11223168145415945189)
XLA Ops:
  0.6 0.8 copy.15
  1.4 0.1 reshape.110
  1.5 0.2 convert_reduce_fusion
  1.7 0.0 copy-start.1
  1.7 0.6 select_reduce_fusion
  2.3 0.1 all_to_all.6
  2.4 9.7 %all_to_all.9 = s32[4,1,4]{2,1,0:T(1,128)S(1)} all-to-all(s32[4,1,4]{2,1,0:T(1,128)S(1)} %bitcast.3), channel_id=1, replica_groups=mesh['st'=4,'tp'=8] {'st'}, dimensions={0} | all-to-all | bytes 128 | tf_op jit(solution)/shard_map/all_to_all | solution.py:398
  12.0 0.5 broadcast.133
  12.5 0.7 reduce.3
  13.2 0.1 reshape.111.ids
  13.3 0.0 copy-start
  13.3 0.5 broadcast_maximum_fusion.ids
  13.8 6.8 %project.1 = bf16[1024,512]{1,0:T(8,128)(2,1)} custom-call(s32[16]{0:T(128)} %broadcast_maximum_fusion.ids, bf16[2048,2048]{1,0:T(8,128)(2,1)} %refs_3_.1, bf16[2048,2048]{1,0:T(8,128)(2,1)} %refs_3_.1, bf16[2048,2048]{1,0:T(8,128)(2,1)} %refs_3_.1, bf16[2048,2048]{1,0:T(8,128)(2,1)} %refs_3_.1, bf16[2048,256]{1,0:T(8,128)(2,1)} %w_k_h.1, ...), custom_call_target="tpu_custom_call" | custom-call | tf_op jit(solution)/shard_map/project/pallas_call | solution.py:50
  20.7 0.0 copy-done.1
  20.7 0.0 copy-done
  20.7 65.6 %main.1 = (f32[512,256]{1,0:T(8,128)}, bf16[16,64,256]{2,1,0:T(8,128)(2,1)}, f32[512,256]{1,0:T(8,128)}) custom-call(s32[8]{0:T(128)} %copy-done.1, s32[16]{0:T(128)} %get-tuple-element.15.req_of, bf16[16,64,512]{2,1,0:T(8,128)(2,1)} %bitcast.2, bf16[512,2048]{1,0:T(8,128)(2,1)} %normed_h.1, bf16[2048,256]{1,0:T(8,128)(2,1)} %w_q_h.1, ...), custom_call_target="tpu_custom_call" | custom-call | tf_op jit(solution)/shard_map/main/pallas_call | solution.py:317
  86.3 3.4 %spread.1 = (f32[2048,256]{1,0:T(8,128)}, f32[512,256]{1,0:T(8,128)}, f32[512,256]{1,0:T(8,128)}) custom-call(s32[16]{0:T(128)} %copy-done, bf16[16,64,256]{2,1,0:T(8,128)(2,1)} %get-tuple-element.9.returned, f32[512,256]{1,0:T(8,128)} %get-tuple-element.10.rows, f32[512,256]{1,0:T(8,128)} %get-tuple-element.11.gqw), custom_call_target="tpu_custom_call" | custom-call | tf_op jit(solution)/shard_map/spread/pallas_call | solution.py:368
  (2 shorter events, 0.0 us)
Async XLA Ops:
  1.7 19.0 %copy-start.1 = (s32[8]{0:T(128)}, s32[8]{0:T(128)S(1)}, u32[]{:S(2)}) copy-start(s32[8]{0:T(128)S(1)} %multiply_add_fusion.slot_of) | copy-start | bytes 100
  13.3 7.4 %copy-start = (s32[16]{0:T(128)}, s32[16]{0:T(128)S(1)}, u32[]{:S(2)}) copy-start(s32[16]{0:T(128)S(1)} %reshape.111.ids) | copy-start | bytes 196
